TPU v7x, 32 devices: a whole 2x2x4 slice. The times are simulated.
32 devices in a mesh: fs: 8 (over z, y), tp: 4 (over x, core).
Axes of the slice: x: 2, y: 2, z: 4, core: 2. Of those that a mesh axis runs over, the one named last changes fastest.
Arguments:
- x_next: bfloat16 [1536, 2048], P(('fs', 'tp')), may hold values from -6 to 6
- x_prev: bfloat16 [1536, 2048], P(('fs', 'tp')), may hold values from -6 to 6
- grad_out: bfloat16 [1536, 2048], P(('fs', 'tp')), may hold values from -6 to 6
- gate_w: bfloat16 [2048, 2816], P('fs', 'tp'), may hold values from -0.125 to 0.125
- up_w: bfloat16 [2048, 2816], P('fs', 'tp'), may hold values from -0.125 to 0.125
- down_w: bfloat16 [2816, 2048], P('tp', 'fs'), may hold values from -0.109375 to 0.109375
- acc_gate: float32 [2048, 2816], P('fs', 'tp'), may hold values from -2.5 to 2.5
- acc_up: float32 [2048, 2816], P('fs', 'tp'), may hold values from -2.5 to 2.5
- acc_down: float32 [2816, 2048], P('tp', 'fs'), may hold values from -2.5 to 2.5
Outputs:
- out_next: bfloat16 [1536, 2048], P(('fs', 'tp'))
- saved_hidden: bfloat16 [1536, 2816], P('fs', 'tp')
- grad_input: bfloat16 [1536, 2048], P(('fs', 'tp'))
- new_gate: float32 [2048, 2816], P('fs', 'tp')
- new_up: float32 [2048, 2816], P('fs', 'tp')
- new_down: float32 [2816, 2048], P('tp', 'fs')
All inputs are finite; a program needn't handle non-finite values.
Results may differ from a plain program's by a relative error of at most 0.014.
Values may be sent and summed in bfloat16 or wider, within the bound.
A program may use at most 64 MiB of HBM per device.

v0:
```python
import math

import jax
import jax.numpy as jnp
from jax import lax
from jax.experimental import pallas as pl
from jax.experimental.pallas import tpu as pltpu
from jax.sharding import PartitionSpec as P

MESH = pl.DeviceIdType.MESH
ANY = pl.BlockSpec(memory_space=pl.ANY)


def columns_of(size):
    side = 1
    while 8 * side * side <= size and size % (2 * side) == 0:
        side *= 2
    return side


def contract_rows(left, right):
    return lax.dot_general(
        left, right, (((0,), (0,)), ((), ())), preferred_element_type=jnp.float32
    )


def contract_cols(left, right):
    return lax.dot_general(
        left, right, (((1,), (1,)), ((), ())), preferred_element_type=jnp.float32
    )


def remote(source, target, send, recv, device):
    return pltpu.make_async_remote_copy(
        src_ref=source, dst_ref=target, send_sem=send, recv_sem=recv,
        device_id=device, device_id_type=MESH,
    )


class Spread:
    def __init__(self, fs, owns, fulls, send, recv):
        self.ny = columns_of(fs)
        self.nz = fs // self.ny
        self.fs, self.owns, self.fulls = fs, owns, fulls
        self.send, self.recv = send, recv
        self.f, self.t = lax.axis_index("fs"), lax.axis_index("tp")
        self.z, self.y = self.f // self.ny, lax.rem(self.f, self.ny)

    def flows(self, w, f, source, up, down, act):
        full = self.fulls[w].at[f]

        def go(kind, z, y):
            act(remote(source, full, self.send.at[w, kind, f], self.recv.at[w, f],
                       (z * self.ny + y, self.t)))

        if up:
            pl.when(self.z + 1 < self.nz)(lambda: go(0, self.z + 1, self.y))
        if down:
            pl.when(self.z > 0)(lambda: go(1, self.z - 1, self.y))
        for k in range(1, self.ny):
            go(1 + k, self.z, lax.rem(self.y + k, self.ny))

    def start(self):
        for w, own in enumerate(self.owns):
            self.flows(w, self.f, own, True, True, lambda c: c.start())

    def arrived(self, w, f):
        full = self.fulls[w].at[f]
        remote(full, full, self.send.at[w, 0, f], self.recv.at[w, f],
               (self.f, self.t)).wait_recv()

    def relay(self, act, wait):
        for d in range(1, self.nz):
            for w in range(len(self.owns)):
                def from_below(w=w, d=d):
                    f = (self.z - d) * self.ny + self.y
                    if wait:
                        self.arrived(w, f)
                    self.flows(w, f, self.fulls[w].at[f], True, False, act)

                def from_above(w=w, d=d):
                    f = (self.z + d) * self.ny + self.y
                    if wait:
                        self.arrived(w, f)
                    self.flows(w, f, self.fulls[w].at[f], False, True, act)

                pl.when(self.z >= d)(from_below)
                pl.when(self.z + d < self.nz)(from_above)

    def finish(self):
        for w in range(len(self.owns)):
            for z in range(self.nz):
                for k in range(1, self.ny):
                    self.arrived(w, z * self.ny + lax.rem(self.y + k, self.ny))
        for w, own in enumerate(self.owns):
            self.flows(w, self.f, own, True, True, lambda c: c.wait_send())
        self.relay(lambda c: c.wait_send(), False)


def stage_in(pairs, sem):
    copies = [pltpu.make_async_copy(a, b, sem.at[i]) for i, (a, b) in enumerate(pairs)]
    for copy in copies:
        copy.start()
    return copies


def gather_inputs(fs, tp, *refs):
    (gate, up, down, xn, xp, go, cols,
     gate_o, up_o, down_o, xn_o, xp_o, go_o, cols_o,
     *rest) = refs
    held, (wsend, wrecv, tsend, trecv, csend, crecv, dsend, drecv, lin, lout) = rest[:7], rest[7:]
    f, t = lax.axis_index("fs"), lax.axis_index("tp")
    sources = (gate, up, down, xn, xp, go, cols)
    into = stage_in(list(zip(sources, held)), lin)
    spread = Spread(fs, held[:3], (gate_o, up_o, down_o), wsend, wrecv)
    for copy in into[:3]:
        copy.wait()
    spread.start()
    for copy in into[3:]:
        copy.wait()
    tokens = ((held[3], xn_o), (held[4], xp_o), (held[5], go_o))
    token_copies = [
        remote(a, b.at[t], tsend.at[i, k], trecv.at[i, t], (f, lax.rem(t + k, tp)))
        for i, (a, b) in enumerate(tokens) for k in range(1, tp)
    ]
    slices = held[6]
    slice_copies = []
    for k in range(1, fs):
        other = lax.rem(f + k, fs)
        slice_copies.append(
            remote(slices.at[other], cols_o.at[f, t], csend.at[k], crecv.at[f], (other, t)))
    for copy in token_copies + slice_copies:
        copy.start()
    out = stage_in(
        [(held[0], gate_o.at[f]), (held[1], up_o.at[f]), (held[2], down_o.at[f]),
         (held[3], xn_o.at[t]), (held[4], xp_o.at[t]), (held[5], go_o.at[t]),
         (slices.at[f], cols_o.at[f, t])], lout)
    spread.relay(lambda c: c.start(), True)
    out[6].wait()
    for k in range(1, fs):
        other = lax.rem(f + k, fs)
        mine = cols_o.at[other, t]
        remote(mine, mine, csend.at[k], crecv.at[other], (f, t)).wait_recv()
    mine = cols_o.at[:, t]
    share = [remote(mine, mine, dsend.at[k], drecv.at[t], (f, lax.rem(t + k, tp)))
             for k in range(1, tp)]
    for copy in share:
        copy.start()
    for k in range(1, tp):
        other = lax.rem(t + k, tp)
        for i, (_, b) in enumerate(tokens):
            remote(b.at[other], b.at[other], tsend.at[i, k], trecv.at[i, other], (f, t)).wait_recv()
        theirs = cols_o.at[:, other]
        remote(theirs, theirs, dsend.at[k], drecv.at[other], (f, t)).wait_recv()
    spread.finish()
    for copy in token_copies + slice_copies + share:
        copy.wait_send()
    for copy in out[:6]:
        copy.wait()


def gather_terms(fs, tp, *refs):
    (gg, gu, hp, pn, pp, gg_o, gu_o, hp_o, pn_o, pp_o, *rest) = refs
    held, (wsend, wrecv, tsend, trecv, lin, lout) = rest[:5], rest[5:]
    f, t = lax.axis_index("fs"), lax.axis_index("tp")
    into = stage_in(list(zip((gg, gu, hp, pn, pp), held)), lin)
    spread = Spread(fs, held[:3], (gg_o, gu_o, hp_o), wsend, wrecv)
    for copy in into[:3]:
        copy.wait()
    spread.start()
    for copy in into[3:]:
        copy.wait()
    parts = ((held[3], pn_o), (held[4], pp_o))
    part_copies = []
    for i, (a, b) in enumerate(parts):
        for k in range(1, tp):
            other = lax.rem(t + k, tp)
            part_copies.append(
                remote(a.at[other], b.at[t], tsend.at[i, k], trecv.at[i, t], (f, other)))
    for copy in part_copies:
        copy.start()
    out = stage_in(
        [(held[0], gg_o.at[f]), (held[1], gu_o.at[f]), (held[2], hp_o.at[f]),
         (held[3].at[t], pn_o.at[t]), (held[4].at[t], pp_o.at[t])], lout)
    spread.relay(lambda c: c.start(), True)
    for i, (_, b) in enumerate(parts):
        for k in range(1, tp):
            other = lax.rem(t + k, tp)
            remote(b.at[other], b.at[other], tsend.at[i, k], trecv.at[i, other], (f, t)).wait_recv()
    spread.finish()
    for copy in part_copies:
        copy.wait_send()
    for copy in out:
        copy.wait()


def communicate(body, fs, tp, args, shapes, extra, name):
    n = len(args)
    return pl.pallas_call(
        lambda *refs: body(fs, tp, *refs),
        out_shape=[jax.ShapeDtypeStruct(s, jnp.bfloat16) for s in shapes],
        in_specs=[ANY] * n,
        out_specs=[ANY] * len(shapes),
        scratch_shapes=[pltpu.VMEM(a.shape, a.dtype) for a in args]
        + [pltpu.SemaphoreType.DMA((3, columns_of(fs) + 1, fs)), pltpu.SemaphoreType.DMA((3, fs)),
           pltpu.SemaphoreType.DMA((3, tp)), pltpu.SemaphoreType.DMA((3, tp))]
        + extra
        + [pltpu.SemaphoreType.DMA((n,)), pltpu.SemaphoreType.DMA((n,))],
        compiler_params=pltpu.CompilerParams(has_side_effects=True),
        name=name,
    )(*args)


def local(x_next, x_prev, grad_out, gate_w, up_w, down_w, acc_gate, acc_up, acc_down):
    fs, tp = lax.axis_size("fs"), lax.axis_size("tp")
    rows, model = x_prev.shape
    depth, width = gate_w.shape
    factor = 1.0 / math.sqrt(rows * tp * fs)
    cols = jnp.concatenate(
        (x_prev.reshape(rows, fs, depth), grad_out.reshape(rows, fs, depth)), axis=2
    ).transpose(1, 0, 2)
    sems = pltpu.SemaphoreType.DMA
    gate_full, up_full, down_full, piece, rows_prev, cotangent, all_cols = communicate(
        gather_inputs, fs, tp, (gate_w.T, up_w.T, down_w, x_next, x_prev, grad_out, cols),
        [(fs, width, depth)] * 3
        + [(tp, rows, model)] * 3 + [(fs, tp, rows, 2 * depth)],
        [sems((fs,)), sems((fs,)), sems((tp,)), sems((tp,))], "gather_inputs",
    )
    gate_full, up_full, down_full = (
        a.transpose(1, 0, 2).reshape(width, model) for a in (gate_full, up_full, down_full)
    )
    piece, rows_prev, cotangent = (a.reshape(tp * rows, model) for a in (piece, rows_prev, cotangent))
    x_cols = all_cols[..., :depth].reshape(fs * tp * rows, depth)
    g_cols = all_cols[..., depth:].reshape(fs * tp * rows, depth)

    gate, upper = contract_cols(piece, gate_full), contract_cols(piece, up_full)
    hidden = (jax.nn.silu(gate) * upper).astype(jnp.bfloat16)
    part_next = jnp.dot(hidden, down_full, preferred_element_type=jnp.float32).astype(jnp.bfloat16)
    gate_prev, up_prev = contract_cols(rows_prev, gate_full), contract_cols(rows_prev, up_full)
    grad_hidden = contract_cols(cotangent, down_full)
    sigmoid_gate = jax.nn.sigmoid(gate_prev)
    silu_gate = gate_prev * sigmoid_gate
    grad_gate = (
        grad_hidden * up_prev * sigmoid_gate * (1.0 + gate_prev * (1.0 - sigmoid_gate))
    ).astype(jnp.bfloat16)
    grad_up = (grad_hidden * silu_gate).astype(jnp.bfloat16)
    hidden_prev = (silu_gate * up_prev).astype(jnp.bfloat16)
    part_prev = (
        jnp.dot(grad_gate, gate_full, preferred_element_type=jnp.float32)
        + jnp.dot(grad_up, up_full, preferred_element_type=jnp.float32)
    ).astype(jnp.bfloat16)

    all_gate, all_up, all_hidden, parts_next, parts_prev = communicate(
        gather_terms, fs, tp,
        (grad_gate, grad_up, hidden_prev,
         part_next.reshape(tp, rows, model), part_prev.reshape(tp, rows, model)),
        [(fs, tp * rows, width)] * 3 + [(tp, rows, model)] * 2, [], "gather_terms",
    )
    all_gate, all_up, all_hidden = (a.reshape(fs * tp * rows, width) for a in (all_gate, all_up, all_hidden))
    new_gate = acc_gate + factor * contract_rows(x_cols, all_gate)
    new_up = acc_up + factor * contract_rows(x_cols, all_up)
    new_down = acc_down + factor * contract_rows(all_hidden, g_cols)
    summed = parts_next.astype(jnp.float32).sum(0).astype(jnp.bfloat16)
    grad_input = parts_prev.astype(jnp.float32).sum(0).astype(jnp.bfloat16)
    return (summed, hidden, grad_input, new_gate, new_up, new_down)


def solution(mesh):
    in_specs = (
        P(("fs", "tp"), None),
        P(("fs", "tp"), None),
        P(("fs", "tp"), None),
        P("fs", "tp"),
        P("fs", "tp"),
        P("tp", "fs"),
        P("fs", "tp"),
        P("fs", "tp"),
        P("tp", "fs"),
    )
    out_specs = (
        P(("fs", "tp"), None),
        P("fs", "tp"),
        P(("fs", "tp"), None),
        P("fs", "tp"),
        P("fs", "tp"),
        P("tp", "fs"),
    )
    return jax.shard_map(local, mesh=mesh, in_specs=in_specs, out_specs=out_specs, check_vma=False)
```

profile of v0, /device:TPU:1, one launch (start us, length us, event | category | flops | bytes accessed | tf_op | source)
XLA Modules:
  0.0 225.6 jit_solution(10953483635780078426)
XLA Ops:
  0.6 1.1 copy_bitcast_fusion
  1.7 0.8 maximum_bitcast_fusion.refs_6_
  2.5 108.7 %gather_inputs.1 = (bf16[8,704,256]{2,1,0:T(8,128)(2,1)}, bf16[8,704,256]{2,1,0:T(8,128)(2,1)}, bf16[8,704,256]{2,1,0:T(8,128)(2,1)}, bf16[4,48,2048]{2,1,0:T(8,...) custom-call(bf16[704,256]{1,0:T(8,128)(2,1)} %bitcast.76, ...), custom_call_target="tpu_custom_call" | custom-call | tf_op jit(solution)/shard_map/gather_inputs/pallas_call | solution.py:199
  111.2 0.0 copy-start.8
  111.2 2.3 %copy.22 = bf16[8,88,8,256]{3,2,0,1:T(8,128)(2,1)S(1)} copy(bf16[8,88,8,256]{3,2,1,0:T(8,128)(2,1)} %bitcast.65) | data formatting | bytes 5767168 | tf_op jit(solution)/shard_map/reshape | solution.py:230
  113.4 0.0 copy-start.4
  113.5 0.0 copy-done.8
  113.5 1.0 fusion.7
  114.5 0.4 copy-done.4
  114.9 0.2 fusion.6
  115.0 0.7 copy-done.1
  115.8 0.4 copy.23
  116.2 1.4 copy-done
  117.6 0.4 copy.24
  118.0 0.7 copy-done.7
  118.7 1.0 fusion.9
  119.7 1.0 fusion.4
  120.8 0.0 copy-start.11
  120.8 1.7 convolution_convert_fusion
  122.5 1.0 fusion.8
  123.6 1.9 multiply_convert_fusion
  125.5 0.8 fusion.10
  126.2 0.0 copy-start.12
  126.2 1.8 fusion
  128.0 0.0 copy-done.5
  128.0 85.6 %gather_terms.1 = (bf16[8,192,704]{2,1,0:T(8,128)(2,1)}, bf16[8,192,704]{2,1,0:T(8,128)(2,1)}, bf16[8,192,704]{2,1,0:T(8,128)(2,1)}, bf16[4,48,2048]{2,1,0:T(8,128)(2,1)}, bf16[4,48,2048]{2,1,0:T(8,128)(2,1)}) custom-call(bf16[192,704]{1,0:T(8,128)(2,1)} %copy-done.5, bf16[192,704]{1,0:T(8,128)(2,1)} %copy-done.3, ...), custom_call_target="tpu_custom_call" | custom-call | tf_op jit(solution)/shard_map/gather_terms/pallas_call | solution.py:199
  213.6 3.4 %fusion.1 = f32[704,256]{1,0:T(8,128)} fusion(f32[704,256]{1,0:T(8,128)S(1)} %copy-done.12, bf16[1536,704]{1,0:T(8,128)(2,1)} %bitcast.78, bf16[1536,256]{1,0:T(8,128)(2,1)S(1)} %bitcast.73), kind=kOutput, calls=%fused_computation.4 | convolution fusion | flops 554008576 | bytes 4390912 | tf_op jit(solution)/shard_map/dot_general | solution.py:22
  217.0 0.8 reduce_sum.24
  217.8 2.1 reduce_sum.25
  220.0 3.8 %fusion.3 = f32[256,704]{0,1:T(8,128)} fusion(f32[256,704]{0,1:T(8,128)} %param.15, bf16[1536,256]{1,0:T(8,128)(2,1)S(1)} %bitcast.59, bf16[1536,704]{1,0:T(8,128)(2,1)} %bitcast.67), kind=kOutput, calls=%fused_computation.8 | convolution fusion | flops 554008576 | bytes 4390912 | tf_op jit(solution)/shard_map/dot_general | solution.py:22
  223.8 0.0 copy-done.10
  223.8 1.9 fusion.2
  (15 shorter events, 0.0 us)
Async XLA Ops:
  111.2 2.3 %copy-start.8 = (bf16[4,48,2048]{2,1,0:T(8,128)(2,1)S(1)}, bf16[4,48,2048]{2,1,0:T(8,128)(2,1)}, u32[]{:S(2)}) copy-start(bf16[4,48,2048]{2,1,0:T(8,128)(2,1)} %get-tuple-element.18) | copy-start | bytes 2359300
  113.4 1.4 copy-start.4
  113.5 2.3 %copy-start.1 = (bf16[8,704,256]{2,1,0:T(8,128)(2,1)S(1)}, bf16[8,704,256]{2,1,0:T(8,128)(2,1)}, u32[]{:S(2)}) copy-start(bf16[8,704,256]{2,1,0:T(8,128)(2,1)} %get-tuple-element.21) | copy-start | bytes 8650756
  115.8 1.8 copy-start
  117.6 1.1 copy-start.7
  120.8 2.8 %copy-start.11 = (bf16[192,704]{1,0:T(8,128)(2,1)}, bf16[192,704]{1,0:T(8,128)(2,1)S(1)}, u32[]{:S(2)}) copy-start(bf16[192,704]{1,0:T(8,128)(2,1)S(1)} %fusion.4) | copy-start | bytes 811012
  120.8 1.7 copy-start.6
  125.4 2.6 %copy-start.3 = (bf16[192,704]{1,0:T(8,128)(2,1)}, bf16[192,704]{1,0:T(8,128)(2,1)S(1)}, u32[]{:S(2)}) copy-start(bf16[192,704]{1,0:T(8,128)(2,1)S(1)} %get-tuple-element.34.refs_1_) | copy-start | bytes 811012
  125.4 2.6 %copy-start.5 = (bf16[192,704]{1,0:T(8,128)(2,1)}, bf16[192,704]{1,0:T(8,128)(2,1)S(1)}, u32[]{:S(2)}) copy-start(bf16[192,704]{1,0:T(8,128)(2,1)S(1)} %get-tuple-element.33.refs_0_) | copy-start | bytes 811012
  126.2 87.4 %copy-start.12 = (f32[704,256]{1,0:T(8,128)S(1)}, f32[704,256]{1,0:T(8,128)}, u32[]{:S(2)}) copy-start(f32[704,256]{1,0:T(8,128)} %param.17) | copy-start | bytes 2162692
  213.6 3.4 %copy-start.9 = (bf16[4,48,2048]{2,1,0:T(8,128)(2,1)S(1)}, bf16[4,48,2048]{2,1,0:T(8,128)(2,1)}, u32[]{:S(2)}) copy-start(bf16[4,48,2048]{2,1,0:T(8,128)(2,1)} %get-tuple-element.24) | copy-start | bytes 2359300
  217.8 5.9 %copy-start.2 = (bf16[8,192,704]{2,1,0:T(8,128)(2,1)S(1)}, bf16[8,192,704]{2,1,0:T(8,128)(2,1)}, u32[]{:S(2)}) copy-start(bf16[8,192,704]{2,1,0:T(8,128)(2,1)} %get-tuple-element.28) | copy-start | bytes 6488068
  220.0 3.8 %copy-start.10 = (f32[256,704]{0,1:T(8,128)S(1)}, f32[256,704]{0,1:T(8,128)}, u32[]{:S(2)}) copy-start(f32[256,704]{0,1:T(8,128)} %param.16) | copy-start | bytes 2162692
where the time goes:
time: 227 us; the launch traced here: 226 us
  Pallas kernels  194 us (85%)
  matrix products  19.3 us (9%)
  local copies, waits for them, and re-layouts  7.55 us (3%)
  other arithmetic  3.74 us (2%)
    pallas_call x2, Pallas kernels, communicate(): pl.pallas_call(lambda *refs: body(fs, tp, *refs), out_shape=[jax.ShapeDty...  194 us
    dot_general x3, matrix products, contract_rows(): lax.dot_general(left, right, (((0,), (0,)), ((), ())), preferred_element_...  9.04 us
    dot_general x5, matrix products, contract_cols(): lax.dot_general(left, right, (((1,), (1,)), ((), ())), preferred_element_...  5.95 us

commit v1 on v0

--- a/solution.py
+++ b/solution.py
@@ -265,6 +265,414 @@
     return (summed, hidden, grad_input, new_gate, new_up, new_down)
 
 
+def step_kernel(nz, ny, nx, *refs):
+    (gate, up, down, xn, xp, go,
+     out_o, gin_o, hid_o, terms_o,
+     W, X, C, AT, AN, G, U, hn, P, Q, S, T, O, DW, DP,
+     wsend, wrecv, ysend, tsend, trecv, csend, crecv, fsend, frecv,
+     gsend, grecv, psend, precv, qsend, qrecv, hsend, hrecv, dsend, drecv, osem) = refs
+    fs, tp = nz * ny, 2 * nx
+    nh, groups, blocks = nz // 2, nz // 2 * ny, 2 * nx
+    width, depth = gate.shape
+    half = width // 2
+    rows, model = xp.shape
+    layer = tp * rows
+    f, t = lax.axis_index("fs"), lax.axis_index("tp")
+    z, y = f // ny, lax.rem(f, ny)
+    x, c = t // 2, lax.rem(t, 2)
+    h, l = z // 2, lax.rem(z, 2)
+    pair = z + 1 - 2 * l
+    mine, group = l * tp + t, h * ny + y
+
+    def dev(x, y, z, c):
+        return (z * ny + y, x * 2 + c)
+
+    here = dev(x, y, z, c)
+    sibling = dev(x, y, z, 1 - c)
+    pending = []
+
+    def send(cond, source, target, ssem, rsem, device):
+        def start():
+            remote(source, target, ssem, rsem, device).start()
+
+        if cond is None:
+            start()
+        else:
+            pl.when(cond)(start)
+        pending.append((cond, source, target, ssem, rsem, device))
+
+    def arrived(ref, ssem, rsem):
+        remote(ref, ref, ssem, rsem, here).wait_recv()
+
+    def around(size, at):
+        return [lax.rem(at + k, size) for k in range(1, size)]
+
+    tokens = (xp, go, xn)
+
+    def block(i):
+        return pl.ds(pl.multiple_of(i * rows, 16), rows)
+
+    def token_targets(first):
+        out = [(1, sibling)]
+        if first:
+            out = [(0, dev(x, y, pair, c))] + [
+                (1 + k, dev(lax.rem(x + k, nx), y, z, c)) for k in range(1, nx)] + out
+        return out
+
+    for m in range(3):
+        pltpu.make_async_copy(tokens[m], X.at[m, block(mine)], trecv.at[m, mine]).start()
+        for kind, device in token_targets(True):
+            send(None, tokens[m], X.at[m, block(mine)], tsend.at[m, mine, kind],
+                 trecv.at[m, mine], device)
+
+    mats = (gate, up, down)
+
+    def rows_of(m, cc):
+        return mats[m].at[pl.ds(pl.multiple_of(cc * half, 16), half)]
+
+    def own_layer():
+        for m in range(3):
+            pltpu.make_async_copy(rows_of(m, c), W.at[m, f], wrecv.at[m, f]).start()
+
+    pl.when(c == l)(own_layer)
+    for m in range(3):
+        send(c == l, rows_of(m, 1 - c), W.at[m, f], wsend.at[m, z, 1 - c], wrecv.at[m, f], sibling)
+    for d in range(nz - 1, 0, -1):
+        for m in range(3):
+            for zc, inside in ((z + d, z + d < nz), (z - d, z - d >= 0)):
+                for cc in range(2):
+                    send(jnp.logical_and(inside, lax.rem(zc + 2 * nz, 2) == c),
+                         rows_of(m, cc), W.at[m, f], wsend.at[m, lax.rem(zc + 2 * nz, nz), cc],
+                         wrecv.at[m, f], dev(x, y, zc, cc))
+
+    others = [(dh, dy) for dh in range(nh) for dy in range(ny) if dh or dy]
+    for dh, dy in others:
+        hh, yy = lax.rem(h + dh, nh), lax.rem(y + dy, ny)
+        for m in range(2):
+            for ls in range(2):
+                at = ((2 * hh + ls) * ny + yy) * depth
+                send(None, tokens[m].at[:, pl.ds(pl.multiple_of(at, 128), depth)],
+                     C.at[2 * m + ls, group, block(mine)],
+                     csend.at[2 * m + ls, hh * ny + yy], crecv.at[2 * m + ls, group],
+                     dev(x, yy, 2 * hh + l, c))
+
+    def forward_weight(m, zz):
+        s = zz * ny + y
+        arrived(W.at[m, s], ysend.at[m, zz, 0], wrecv.at[m, s])
+        for k in range(1, ny):
+            remote(W.at[m, s], W.at[m, s], ysend.at[m, zz, k], wrecv.at[m, s],
+                   dev(x, lax.rem(y + k, ny), z, c)).start()
+
+    def forward_token(i, first):
+        for m in range(3):
+            arrived(X.at[m, block(i)], tsend.at[m, i, 0], trecv.at[m, i])
+            for kind, device in token_targets(True)[1:] if first else token_targets(False):
+                send(None, X.at[m, block(i)], X.at[m, block(i)], tsend.at[m, i, kind],
+                     trecv.at[m, i], device)
+
+    def forward_column(m, step):
+        for d in step:
+            pl.when(z + d < nz)(lambda d=d: forward_weight(m, z + d))
+            pl.when(z - d >= 0)(lambda d=d: forward_weight(m, z - d))
+
+    for m in range(3):
+        forward_weight(m, z)
+    forward_token((1 - l) * tp + t, True)
+    for xx in around(nx, x):
+        forward_token(l * tp + xx * 2 + c, False)
+    forward_column(0, range(1, nz))
+    for xx in around(nx, x):
+        forward_token((1 - l) * tp + xx * 2 + c, False)
+    forward_column(1, range(1, nz))
+    forward_column(2, range(1, nz))
+
+    for m in range(3):
+        arrived(X.at[m, block(mine)], tsend.at[m, mine, 0], trecv.at[m, mine])
+        for ll in range(2):
+            for xx in range(nx):
+                i = ll * tp + xx * 2 + 1 - c
+                arrived(X.at[m, block(i)], tsend.at[m, i, 0], trecv.at[m, i])
+
+    AT[...] = jnp.zeros_like(AT)
+    AN[...] = jnp.zeros_like(AN)
+
+    def slice_products(s):
+        at = pl.ds(pl.multiple_of(s * depth, 128), depth)
+        p, g, n = X[0, :, at], X[1, :, at], X[2, :, at]
+        AT[0] += contract_cols(W[0, s], p)
+        AT[1] += contract_cols(W[1, s], p)
+        AT[2] += contract_cols(W[2, s], g)
+        AN[0] += contract_cols(n, W[0, s])
+        AN[1] += contract_cols(n, W[1, s])
+
+    def own_column(k, carry):
+        slice_products(k * ny + y)
+        return carry
+
+    lax.fori_loop(0, nz, own_column, 0)
+
+    def other_column(yy, k, carry):
+        s = lax.rem(z + k, nz) * ny + yy
+        for m in range(3):
+            arrived(W.at[m, s], ysend.at[m, 0, 0], wrecv.at[m, s])
+        slice_products(s)
+        return carry
+
+    for yy in around(ny, y):
+        lax.fori_loop(0, nz, lambda k, carry, yy=yy: other_column(yy, k, carry), 0)
+
+    part = math.gcd(half, 32)
+
+    def gradients(r, carry):
+        at = pl.ds(pl.multiple_of(r * part, part), part)
+        g, u, gh = AT[0, at], AT[1, at], AT[2, at]
+        s = jax.nn.sigmoid(g)
+        sg = g * s
+        G[0, group, at] = (gh * u * s * (1.0 + g * (1.0 - s))).astype(jnp.bfloat16)
+        G[1, group, at] = (gh * sg).astype(jnp.bfloat16)
+        G[2, group, at] = (sg * u).astype(jnp.bfloat16)
+        return carry
+
+    lax.fori_loop(0, half // part, gradients, 0)
+    step = math.gcd(rows, 32)
+
+    def activations(r, carry):
+        at = pl.ds(pl.multiple_of(r * step, step), step)
+        g = AN[0, at]
+        hn[at] = (g * jax.nn.sigmoid(g) * AN[1, at]).astype(jnp.bfloat16)
+        return carry
+
+    lax.fori_loop(0, 2 * layer // step, activations, 0)
+
+    for m in range(3):
+        for k in range(1, nh):
+            hh = lax.rem(h + k, nh)
+            send(None, G.at[m, group], G.at[m, group], gsend.at[m, group, k - 1],
+                 grecv.at[m, group], dev(x, y, 2 * hh + l, c))
+        for k in range(1, ny):
+            send(None, G.at[m, group], G.at[m, group], gsend.at[m, group, nh + k - 1],
+                 grecv.at[m, group], dev(x, lax.rem(y + k, ny), z, c))
+
+    for ll in range(2):
+        source = hn.at[pl.ds(ll * layer, layer)]
+        alone = jnp.logical_and(l == ll, c == l)
+        pl.when(alone)(lambda source=source: pltpu.make_async_copy(
+            source, hid_o.at[c], hrecv.at[c]).start())
+        send(jnp.logical_not(alone), source, hid_o.at[c], hsend.at[ll], hrecv.at[c],
+             dev(x, y, 2 * h + ll, l))
+
+    def column_targets(first):
+        return [(kind, device) for kind, device in token_targets(first)]
+
+    def forward_columns(i, targets, direct):
+        for dh, dy in others:
+            g = lax.rem(h + dh, nh) * ny + lax.rem(y + dy, ny)
+            if direct:
+                for j in range(4):
+                    arrived(C.at[j, g, block(i)], csend.at[j, g], crecv.at[j, g])
+            else:
+                arrived(C.at[:, g, block(i)], fsend.at[g, i, 0], frecv.at[g, i])
+            for kind, device in targets:
+                send(None, C.at[:, g, block(i)], C.at[:, g, block(i)], fsend.at[g, i, kind],
+                     frecv.at[g, i], device)
+
+    forward_columns(mine, token_targets(True), True)
+
+    U[0] = G[0, group].T
+    U[1] = G[1, group].T
+
+    def shares(s, carry):
+        at = pl.ds(pl.multiple_of(s * depth, 128), depth)
+        P[0, :, at] = jnp.dot(
+            hn[...], W[2, s], preferred_element_type=jnp.float32).astype(jnp.bfloat16)
+        P[1, :, at] = (
+            jnp.dot(U[0], W[0, s], preferred_element_type=jnp.float32)
+            + jnp.dot(U[1], W[1, s], preferred_element_type=jnp.float32)
+        ).astype(jnp.bfloat16)
+        return carry
+
+    lax.fori_loop(0, fs, shares, 0)
+
+    forward_columns((1 - l) * tp + t, token_targets(True)[1:], False)
+    for ll in range(2):
+        for xx in range(nx):
+            i = ll * tp + xx * 2 + 1 - c
+            for p in range(2):
+                send(None, P.at[p, block(i)], Q.at[p, ll * nx + xx], psend.at[p, ll * nx + xx],
+                     precv.at[p, ll * nx + xx], sibling)
+
+    for m in range(2):
+        for ls in range(2):
+            at = ((2 * h + ls) * ny + y) * depth
+            C[2 * m + ls, group] = X[m, :, pl.ds(pl.multiple_of(at, 128), depth)]
+
+    def weight_terms(m, g, first):
+        for ls in range(2):
+            value = jnp.dot(G[m, g], C[(2 if m == 2 else 0) + ls, g],
+                            preferred_element_type=jnp.float32)
+            if first:
+                DW[ls, m] = value
+            else:
+                DW[ls, m] += value
+
+    for m in range(3):
+        weight_terms(m, group, True)
+
+    spot = l * nx + x
+    for ll in range(2):
+        for xx in range(nx):
+            b = ll * nx + xx
+            i = ll * tp + xx * 2 + c
+            for p in range(2):
+                arrived(Q.at[p, b], psend.at[p, b], precv.at[p, b])
+                S[p, b] = (P[p, block(i)].astype(jnp.float32)
+                           + Q[p, b].astype(jnp.float32)).astype(jnp.bfloat16)
+    for ll in range(2):
+        for xx in range(nx):
+            b = ll * nx + xx
+            for p in range(2):
+                send(b != spot, S.at[p, b], T.at[p, spot], qsend.at[p, b], qrecv.at[p, spot],
+                     dev(xx, y, 2 * h + ll, c))
+
+    for xx in around(nx, x):
+        forward_columns(l * tp + xx * 2 + c, token_targets(False), False)
+        forward_columns((1 - l) * tp + xx * 2 + c, token_targets(False), False)
+    for ll in range(2):
+        for xx in range(nx):
+            i = ll * tp + xx * 2 + 1 - c
+            for dh, dy in others:
+                g = lax.rem(h + dh, nh) * ny + lax.rem(y + dy, ny)
+                arrived(C.at[:, g, block(i)], fsend.at[g, i, 0], frecv.at[g, i])
+
+    def relay_terms(m):
+        for k in range(1, nh):
+            g = lax.rem(h + k, nh) * ny + y
+            arrived(G.at[m, g], gsend.at[m, g, 0], grecv.at[m, g])
+            for j in range(1, ny):
+                send(None, G.at[m, g], G.at[m, g], gsend.at[m, g, nh + j - 1], grecv.at[m, g],
+                     dev(x, lax.rem(y + j, ny), z, c))
+
+    relay_terms(0)
+    for m in range(3):
+        for k in range(1, nh):
+            weight_terms(m, lax.rem(h + k, nh) * ny + y, False)
+        for j in range(1, ny):
+            g = h * ny + lax.rem(y + j, ny)
+            arrived(G.at[m, g], gsend.at[m, g, 0], grecv.at[m, g])
+            weight_terms(m, g, False)
+        if m + 1 < 3:
+            relay_terms(m + 1)
+        for k in range(1, nh):
+            for j in range(1, ny):
+                g = lax.rem(h + k, nh) * ny + lax.rem(y + j, ny)
+                arrived(G.at[m, g], gsend.at[m, g, 0], grecv.at[m, g])
+                weight_terms(m, g, False)
+        DP[0, m] = DW[1 - l, m].astype(jnp.bfloat16)
+        DP[1, m] = DW[l, m].astype(jnp.bfloat16)
+        send(None, DP.at[0, m], terms_o.at[c, m], dsend.at[0, m], drecv.at[c, m],
+             dev(x, y, pair, l))
+        pl.when(c == l)(lambda m=m: pltpu.make_async_copy(
+            DP.at[1, m], terms_o.at[c, m], drecv.at[c, m]).start())
+        send(c != l, DP.at[1, m], terms_o.at[c, m], dsend.at[1, m], drecv.at[c, m], sibling)
+
+    for p in range(2):
+        total = S[p, spot].astype(jnp.float32)
+        for b in range(blocks):
+            pl.when(b != spot)(lambda p=p, b=b: arrived(
+                T.at[p, b], qsend.at[p, b], qrecv.at[p, b]))
+        for k in range(1, blocks):
+            total += T[p, lax.rem(spot + k, blocks)].astype(jnp.float32)
+        O[p] = total.astype(jnp.bfloat16)
+    results = [pltpu.make_async_copy(O.at[p], ref, osem.at[p])
+               for p, ref in enumerate((out_o, gin_o))]
+
+    for cond, *copy in pending:
+        def finish(copy=copy):
+            remote(*copy).wait_send()
+
+        if cond is None:
+            finish()
+        else:
+            pl.when(cond)(finish)
+    for copy in results:
+        copy.start()
+    for m in range(3):
+        for zz in range(nz):
+            s = zz * ny + y
+            for k in range(1, ny):
+                remote(W.at[m, s], W.at[m, s], ysend.at[m, zz, k], wrecv.at[m, s],
+                       dev(x, lax.rem(y + k, ny), z, c)).wait_send()
+    for cc in range(2):
+        arrived(hid_o.at[cc], hsend.at[cc], hrecv.at[cc])
+        for m in range(3):
+            arrived(terms_o.at[cc, m], dsend.at[0, m], drecv.at[cc, m])
+    for copy in results:
+        copy.wait()
+
+
+def layered(x_next, x_prev, grad_out, gate_w, up_w, down_w, acc_gate, acc_up, acc_down):
+    fs, tp = lax.axis_size("fs"), lax.axis_size("tp")
+    ny = columns_of(fs)
+    nz, nx = fs // ny, tp // 2
+    rows, model = x_prev.shape
+    depth, width = gate_w.shape
+    half, tokens = width // 2, 2 * tp * rows
+    groups, blocks = nz // 2 * ny, 2 * nx
+    factor = 1.0 / math.sqrt(rows * tp * fs)
+    bf, sems = jnp.bfloat16, pltpu.SemaphoreType.DMA
+    out_next, grad_input, hidden, terms = pl.pallas_call(
+        lambda *refs: step_kernel(nz, ny, nx, *refs),
+        out_shape=[jax.ShapeDtypeStruct(s, bf) for s in (
+            (rows, model), (rows, model), (2, tp * rows, half), (2, 3, half, depth))],
+        in_specs=[ANY] * 6,
+        out_specs=[ANY] * 4,
+        scratch_shapes=[
+            pltpu.VMEM((3, fs, half, depth), bf),
+            pltpu.VMEM((3, tokens, model), bf),
+            pltpu.VMEM((4, groups, tokens, depth), bf),
+            pltpu.VMEM((3, half, tokens), jnp.float32),
+            pltpu.VMEM((2, tokens, half), jnp.float32),
+            pltpu.VMEM((3, groups, half, tokens), bf),
+            pltpu.VMEM((2, tokens, half), bf),
+            pltpu.VMEM((tokens, half), bf),
+            pltpu.VMEM((2, tokens, model), bf),
+            pltpu.VMEM((2, blocks, rows, model), bf),
+            pltpu.VMEM((2, blocks, rows, model), bf),
+            pltpu.VMEM((2, blocks, rows, model), bf),
+            pltpu.VMEM((2, rows, model), bf),
+            pltpu.VMEM((2, 3, half, depth), jnp.float32),
+            pltpu.VMEM((2, 3, half, depth), bf),
+            sems((3, nz, 2)), sems((3, fs)), sems((3, nz, ny)),
+            sems((3, 2 * tp, nx + 1)), sems((3, 2 * tp)),
+            sems((4, groups)), sems((4, groups)),
+            sems((groups, 2 * tp, nx + 1)), sems((groups, 2 * tp)),
+            sems((3, groups, nz // 2 + ny)), sems((3, groups)),
+            sems((2, blocks)), sems((2, blocks)), sems((2, blocks)), sems((2, blocks)),
+            sems((2,)), sems((2,)), sems((2, 3)), sems((2, 3)), sems((2,)),
+        ],
+        compiler_params=pltpu.CompilerParams(has_side_effects=True),
+        name="step",
+    )(gate_w.T, up_w.T, down_w, x_next, x_prev, grad_out)
+    saved = jnp.concatenate((hidden[0], hidden[1]), axis=1)
+
+    def updated(acc, m):
+        return acc + factor * terms[:, m].reshape(width, depth).astype(jnp.float32)
+
+    return (out_next, saved, grad_input,
+            updated(acc_gate.T, 0).T, updated(acc_up.T, 1).T, updated(acc_down, 2))
+
+
+def layers_fit(fs, tp, rows, depth, width):
+    nz = fs // columns_of(fs)
+    return nz % 2 == 0 and tp % 2 == 0 and depth % 128 == 0 and width % 32 == 0 and rows % 16 == 0
+
+
+def choose(*args):
+    depth, width = args[3].shape
+    fits = layers_fit(lax.axis_size("fs"), lax.axis_size("tp"), args[0].shape[0], depth, width)
+    return (layered if fits else local)(*args)
+
+
 def solution(mesh):
     in_specs = (
         P(("fs", "tp"), None),
@@ -285,4 +693,4 @@
         P("fs", "tp"),
         P("tp", "fs"),
     )
-    return jax.shard_map(local, mesh=mesh, in_specs=in_specs, out_specs=out_specs, check_vma=False)
+    return jax.shard_map(choose, mesh=mesh, in_specs=in_specs, out_specs=out_specs, check_vma=False)

time: 227 us -> 167 us (0.74)
  the two profiles are of different devices: /device:TPU:1 before, /device:TPU:21 now
where the time goes in v1:
time: 167 us
  Pallas kernels  159 us (95%)
  local copies, waits for them, and re-layouts  3.58 us (2%)
  other arithmetic  3.27 us (2%)
    pallas_call x1, Pallas kernels, layered(): pl.pallas_call(lambda *refs: step_kernel(nz, ny, nx, *refs), out_shape=[j...  159 us

profile of v1, /device:TPU:21, one launch (start us, length us, event | category | flops | bytes accessed | tf_op | source)
XLA Modules:
  0.0 166.6 jit_solution(10832257740384898637)
XLA Ops:
  0.6 159.1 %step.1 = (bf16[48,2048]{1,0:T(8,128)(2,1)}, bf16[48,2048]{1,0:T(8,128)(2,1)}, bf16[2,192,352]{2,1,0:T(8,128)(2,1)}, bf16[2,3,352,256]{3,2,1,0:T(8,128)(2,1)}) custom-call(bf16[704,256]{1,0:T(8,128)(2,1)} %bitcast.20, bf16[704,256]{1,0:T(8,128)(2,1)} %bitcast.21, bf16[704,256]{1,0:T(8,128)(2,1)} %refs_2_.1, bf16[48,2048]{1,0:T(8,128)(2,1)} %refs_3_.1, ...), custom_call_target="tpu_custom_call" | custom-call | tf_op jit(solution)/shard_map/step/pallas_call | solution.py:623
  159.8 0.0 copy-start
  159.8 1.1 slice_bitcast_fusion.1
  160.9 0.8 pad_maximum_fusion
  161.7 0.0 copy-done
  161.7 0.0 copy-start.2
  161.7 0.0 copy-start.3
  161.7 0.2 convert_multiply_fusion
  161.9 0.9 copy-done.2
  162.8 0.2 copy-done.3
  163.0 0.0 copy-start.1
  163.0 1.3 bitcast_add_fusion
  164.3 0.0 copy-done.1
  164.3 0.0 copy-start.5
  164.3 0.0 copy-start.4
  164.3 0.9 bitcast_add_fusion.2
  165.3 0.0 copy-done.5
  165.3 0.7 copy.17
  166.0 0.0 copy-done.4
  166.0 0.7 copy.18
Async XLA Ops:
  159.8 2.0 %copy-start = (bf16[2,3,352,256]{3,2,1,0:T(8,128)(2,1)S(1)}, bf16[2,3,352,256]{3,2,1,0:T(8,128)(2,1)}, u32[]{:S(2)}) copy-start(bf16[2,3,352,256]{3,2,1,0:T(8,128)(2,1)} %get-tuple-element.13) | copy-start | bytes 3244036
  161.7 1.1 copy-start.2
  161.7 1.3 copy-start.3
  163.0 1.3 copy-start.1
  164.3 1.0 copy-start.5
  164.3 1.6 copy-start.4

commit v2 on v1

--- a/solution.py
+++ b/solution.py
@@ -307,6 +307,14 @@
     def around(size, at):
         return [lax.rem(at + k, size) for k in range(1, size)]
 
+    barrier = pltpu.get_barrier_semaphore()
+    peers = [dev(x, y, lax.rem(z + d, nz), cc) for d in range(1, nz) for cc in range(2)]
+    peers += [sibling] + [dev(xx, y, z, c) for xx in around(nx, x)]
+    peers += [dev(x, yy, lax.rem(z + 2 * d, nz), c) for yy in around(ny, y) for d in range(nh)]
+    for peer in peers:
+        pl.semaphore_signal(barrier, inc=1, device_id=peer, device_id_type=MESH)
+    pl.semaphore_wait(barrier, len(peers))
+
     tokens = (xp, go, xn)
 
     def block(i):
@@ -326,24 +334,28 @@
                  trecv.at[m, mine], device)
 
     mats = (gate, up, down)
-
-    def rows_of(m, cc):
-        return mats[m].at[pl.ds(pl.multiple_of(cc * half, 16), half)]
+    piece = half // 2
+
+    def rows_of(q, cc):
+        return mats[q // 2].at[pl.ds(pl.multiple_of(cc * half + q % 2 * piece, 16), piece)]
+
+    def slot(q, s):
+        return W.at[q // 2, s, pl.ds(q % 2 * piece, piece)]
 
     def own_layer():
-        for m in range(3):
-            pltpu.make_async_copy(rows_of(m, c), W.at[m, f], wrecv.at[m, f]).start()
+        for q in range(6):
+            pltpu.make_async_copy(rows_of(q, c), slot(q, f), wrecv.at[q, f]).start()
 
     pl.when(c == l)(own_layer)
-    for m in range(3):
-        send(c == l, rows_of(m, 1 - c), W.at[m, f], wsend.at[m, z, 1 - c], wrecv.at[m, f], sibling)
-    for d in range(nz - 1, 0, -1):
-        for m in range(3):
+    for q in range(6):
+        send(c == l, rows_of(q, 1 - c), slot(q, f), wsend.at[q, z, 1 - c], wrecv.at[q, f], sibling)
+    for q in range(6):
+        for d in range(nz - 1, 0, -1):
             for zc, inside in ((z + d, z + d < nz), (z - d, z - d >= 0)):
                 for cc in range(2):
                     send(jnp.logical_and(inside, lax.rem(zc + 2 * nz, 2) == c),
-                         rows_of(m, cc), W.at[m, f], wsend.at[m, lax.rem(zc + 2 * nz, nz), cc],
-                         wrecv.at[m, f], dev(x, y, zc, cc))
+                         rows_of(q, cc), slot(q, f), wsend.at[q, lax.rem(zc + 2 * nz, nz), cc],
+                         wrecv.at[q, f], dev(x, y, zc, cc))
 
     others = [(dh, dy) for dh in range(nh) for dy in range(ny) if dh or dy]
     for dh, dy in others:
@@ -356,11 +368,11 @@
                      csend.at[2 * m + ls, hh * ny + yy], crecv.at[2 * m + ls, group],
                      dev(x, yy, 2 * hh + l, c))
 
-    def forward_weight(m, zz):
+    def forward_weight(q, zz):
         s = zz * ny + y
-        arrived(W.at[m, s], ysend.at[m, zz, 0], wrecv.at[m, s])
+        arrived(slot(q, s), ysend.at[q, zz, 0], wrecv.at[q, s])
         for k in range(1, ny):
-            remote(W.at[m, s], W.at[m, s], ysend.at[m, zz, k], wrecv.at[m, s],
+            remote(slot(q, s), slot(q, s), ysend.at[q, zz, k], wrecv.at[q, s],
                    dev(x, lax.rem(y + k, ny), z, c)).start()
 
     def forward_token(i, first):
@@ -370,22 +382,22 @@
                 send(None, X.at[m, block(i)], X.at[m, block(i)], tsend.at[m, i, kind],
                      trecv.at[m, i], device)
 
-    def forward_column(m, step):
-        for d in step:
-            pl.when(z + d < nz)(lambda d=d: forward_weight(m, z + d))
-            pl.when(z - d >= 0)(lambda d=d: forward_weight(m, z - d))
-
-    for m in range(3):
-        forward_weight(m, z)
+    def forward_column(m):
+        for q in (2 * m, 2 * m + 1):
+            for d in range(1, nz):
+                pl.when(z + d < nz)(lambda q=q, d=d: forward_weight(q, z + d))
+                pl.when(z - d >= 0)(lambda q=q, d=d: forward_weight(q, z - d))
+
+    for q in range(6):
+        forward_weight(q, z)
+    forward_column(0)
     forward_token((1 - l) * tp + t, True)
     for xx in around(nx, x):
         forward_token(l * tp + xx * 2 + c, False)
-    forward_column(0, range(1, nz))
+    forward_column(1)
     for xx in around(nx, x):
         forward_token((1 - l) * tp + xx * 2 + c, False)
-    forward_column(1, range(1, nz))
-    forward_column(2, range(1, nz))
-
+    forward_column(2)
     for m in range(3):
         arrived(X.at[m, block(mine)], tsend.at[m, mine, 0], trecv.at[m, mine])
         for ll in range(2):
@@ -413,8 +425,8 @@
 
     def other_column(yy, k, carry):
         s = lax.rem(z + k, nz) * ny + yy
-        for m in range(3):
-            arrived(W.at[m, s], ysend.at[m, 0, 0], wrecv.at[m, s])
+        for q in range(6):
+            arrived(slot(q, s), ysend.at[q, 0, 0], wrecv.at[q, s])
         slice_products(s)
         return carry
 
@@ -492,8 +504,6 @@
         return carry
 
     lax.fori_loop(0, fs, shares, 0)
-
-    forward_columns((1 - l) * tp + t, token_targets(True)[1:], False)
     for ll in range(2):
         for xx in range(nx):
             i = ll * tp + xx * 2 + 1 - c
@@ -517,8 +527,6 @@
 
     for m in range(3):
         weight_terms(m, group, True)
-
-    spot = l * nx + x
     for ll in range(2):
         for xx in range(nx):
             b = ll * nx + xx
@@ -527,22 +535,12 @@
                 arrived(Q.at[p, b], psend.at[p, b], precv.at[p, b])
                 S[p, b] = (P[p, block(i)].astype(jnp.float32)
                            + Q[p, b].astype(jnp.float32)).astype(jnp.bfloat16)
-    for ll in range(2):
-        for xx in range(nx):
-            b = ll * nx + xx
+    for k in range(1, nx):
+        xx = lax.rem(x + k, nx)
+        for ll in range(2):
             for p in range(2):
-                send(b != spot, S.at[p, b], T.at[p, spot], qsend.at[p, b], qrecv.at[p, spot],
-                     dev(xx, y, 2 * h + ll, c))
-
-    for xx in around(nx, x):
-        forward_columns(l * tp + xx * 2 + c, token_targets(False), False)
-        forward_columns((1 - l) * tp + xx * 2 + c, token_targets(False), False)
-    for ll in range(2):
-        for xx in range(nx):
-            i = ll * tp + xx * 2 + 1 - c
-            for dh, dy in others:
-                g = lax.rem(h + dh, nh) * ny + lax.rem(y + dy, ny)
-                arrived(C.at[:, g, block(i)], fsend.at[g, i, 0], frecv.at[g, i])
+                send(None, S.at[p, ll * nx + xx], T.at[p, ll * nx + x], qsend.at[p, ll * nx + k],
+                     qrecv.at[p, ll * nx + x], dev(xx, y, z, c))
 
     def relay_terms(m):
         for k in range(1, nh):
@@ -553,6 +551,29 @@
                      dev(x, lax.rem(y + j, ny), z, c))
 
     relay_terms(0)
+    forward_columns((1 - l) * tp + t, token_targets(True)[1:], False)
+    for xx in around(nx, x):
+        forward_columns(l * tp + xx * 2 + c, token_targets(False), False)
+        forward_columns((1 - l) * tp + xx * 2 + c, token_targets(False), False)
+    relay_terms(1)
+
+    for ll in (1 - l, l):
+        for p in range(2):
+            total = S[p, ll * nx + x].astype(jnp.float32)
+            for xx in around(nx, x):
+                arrived(T.at[p, ll * nx + xx], qsend.at[p, 0], qrecv.at[p, ll * nx + xx])
+                total += T[p, ll * nx + xx].astype(jnp.float32)
+            O[p, ll] = total.astype(jnp.bfloat16)
+    for p in range(2):
+        send(None, O.at[p, 1 - l], T.at[p, l * nx + x], qsend.at[p, 0], qrecv.at[p, l * nx + x],
+             dev(x, y, pair, c))
+    for ll in range(2):
+        for xx in range(nx):
+            i = ll * tp + xx * 2 + 1 - c
+            for dh, dy in others:
+                g = lax.rem(h + dh, nh) * ny + lax.rem(y + dy, ny)
+                arrived(C.at[:, g, block(i)], fsend.at[g, i, 0], frecv.at[g, i])
+
     for m in range(3):
         for k in range(1, nh):
             weight_terms(m, lax.rem(h + k, nh) * ny + y, False)
@@ -560,8 +581,8 @@
             g = h * ny + lax.rem(y + j, ny)
             arrived(G.at[m, g], gsend.at[m, g, 0], grecv.at[m, g])
             weight_terms(m, g, False)
-        if m + 1 < 3:
-            relay_terms(m + 1)
+        if m == 0:
+            relay_terms(2)
         for k in range(1, nh):
             for j in range(1, ny):
                 g = lax.rem(h + k, nh) * ny + lax.rem(y + j, ny)
@@ -574,16 +595,12 @@
         pl.when(c == l)(lambda m=m: pltpu.make_async_copy(
             DP.at[1, m], terms_o.at[c, m], drecv.at[c, m]).start())
         send(c != l, DP.at[1, m], terms_o.at[c, m], dsend.at[1, m], drecv.at[c, m], sibling)
-
     for p in range(2):
-        total = S[p, spot].astype(jnp.float32)
-        for b in range(blocks):
-            pl.when(b != spot)(lambda p=p, b=b: arrived(
-                T.at[p, b], qsend.at[p, b], qrecv.at[p, b]))
-        for k in range(1, blocks):
-            total += T[p, lax.rem(spot + k, blocks)].astype(jnp.float32)
-        O[p] = total.astype(jnp.bfloat16)
-    results = [pltpu.make_async_copy(O.at[p], ref, osem.at[p])
+        at = (1 - l) * nx + x
+        arrived(T.at[p, at], qsend.at[p, 0], qrecv.at[p, at])
+        O[p, 2] = (O[p, l].astype(jnp.float32)
+                   + T[p, at].astype(jnp.float32)).astype(jnp.bfloat16)
+    results = [pltpu.make_async_copy(O.at[p, 2], ref, osem.at[p])
                for p, ref in enumerate((out_o, gin_o))]
 
     for cond, *copy in pending:
@@ -596,11 +613,11 @@
             pl.when(cond)(finish)
     for copy in results:
         copy.start()
-    for m in range(3):
+    for q in range(6):
         for zz in range(nz):
             s = zz * ny + y
             for k in range(1, ny):
-                remote(W.at[m, s], W.at[m, s], ysend.at[m, zz, k], wrecv.at[m, s],
+                remote(slot(q, s), slot(q, s), ysend.at[q, zz, k], wrecv.at[q, s],
                        dev(x, lax.rem(y + k, ny), z, c)).wait_send()
     for cc in range(2):
         arrived(hid_o.at[cc], hsend.at[cc], hrecv.at[cc])
@@ -608,6 +625,20 @@
             arrived(terms_o.at[cc, m], dsend.at[0, m], drecv.at[cc, m])
     for copy in results:
         copy.wait()
+
+
+def finish_kernel(factor, terms, acc0, acc1, acc2, hidden, a, b, new0, new1, new2, saved, a_o, b_o):
+    for m, (acc, new) in enumerate(((acc0, new0), (acc1, new1), (acc2, new2))):
+        new[...] = acc[...] + factor * terms[0, m].astype(jnp.float32)
+
+    def rest():
+        half = hidden.shape[2]
+        saved[:, pl.ds(0, half)] = hidden[0]
+        saved[:, pl.ds(half, half)] = hidden[1]
+        a_o[...] = a[...]
+        b_o[...] = b[...]
+
+    pl.when(pl.program_id(0) == 0)(rest)
 
 
 def layered(x_next, x_prev, grad_out, gate_w, up_w, down_w, acc_gate, acc_up, acc_down):
@@ -639,10 +670,10 @@
             pltpu.VMEM((2, blocks, rows, model), bf),
             pltpu.VMEM((2, blocks, rows, model), bf),
             pltpu.VMEM((2, blocks, rows, model), bf),
-            pltpu.VMEM((2, rows, model), bf),
+            pltpu.VMEM((2, 3, rows, model), bf),
             pltpu.VMEM((2, 3, half, depth), jnp.float32),
             pltpu.VMEM((2, 3, half, depth), bf),
-            sems((3, nz, 2)), sems((3, fs)), sems((3, nz, ny)),
+            sems((6, nz, 2)), sems((6, fs)), sems((6, nz, ny)),
             sems((3, 2 * tp, nx + 1)), sems((3, 2 * tp)),
             sems((4, groups)), sems((4, groups)),
             sems((groups, 2 * tp, nx + 1)), sems((groups, 2 * tp)),
@@ -650,21 +681,33 @@
             sems((2, blocks)), sems((2, blocks)), sems((2, blocks)), sems((2, blocks)),
             sems((2,)), sems((2,)), sems((2, 3)), sems((2, 3)), sems((2,)),
         ],
-        compiler_params=pltpu.CompilerParams(has_side_effects=True),
+        compiler_params=pltpu.CompilerParams(has_side_effects=True, collective_id=0),
         name="step",
     )(gate_w.T, up_w.T, down_w, x_next, x_prev, grad_out)
-    saved = jnp.concatenate((hidden[0], hidden[1]), axis=1)
-
-    def updated(acc, m):
-        return acc + factor * terms[:, m].reshape(width, depth).astype(jnp.float32)
-
-    return (out_next, saved, grad_input,
-            updated(acc_gate.T, 0).T, updated(acc_up.T, 1).T, updated(acc_down, 2))
+    piece = half // 2
+    piece_spec = pl.BlockSpec((piece, depth), lambda i: (i, 0))
+
+    def whole(*shape):
+        return pl.BlockSpec(shape, lambda i: (0,) * len(shape))
+
+    new_gate, new_up, new_down, saved, out_next, grad_input = pl.pallas_call(
+        lambda *refs: finish_kernel(factor, *refs),
+        grid=(4,),
+        out_shape=[jax.ShapeDtypeStruct((width, depth), jnp.float32)] * 3 + [
+            jax.ShapeDtypeStruct((tp * rows, width), bf)]
+        + [jax.ShapeDtypeStruct((rows, model), bf)] * 2,
+        in_specs=[pl.BlockSpec((1, 3, piece, depth), lambda i: (i // 2, 0, i % 2, 0))]
+        + [piece_spec] * 3 + [whole(2, tp * rows, half), whole(rows, model), whole(rows, model)],
+        out_specs=[piece_spec] * 3
+        + [whole(tp * rows, width), whole(rows, model), whole(rows, model)],
+        name="finish",
+    )(terms, acc_gate.T, acc_up.T, acc_down, hidden, out_next, grad_input)
+    return (out_next, saved, grad_input, new_gate.T, new_up.T, new_down)
 
 
 def layers_fit(fs, tp, rows, depth, width):
     nz = fs // columns_of(fs)
-    return nz % 2 == 0 and tp % 2 == 0 and depth % 128 == 0 and width % 32 == 0 and rows % 16 == 0
+    return nz % 2 == 0 and tp % 2 == 0 and depth % 128 == 0 and width % 64 == 0 and rows % 16 == 0
 
 
 def choose(*args):

time: 167 us -> 138 us (0.83)
  the two profiles are of different devices: /device:TPU:21 before, /device:TPU:1 now
where the time goes in v2:
time: 138 us
  Pallas kernels  137 us (99%)
    pallas_call x1, Pallas kernels, layered(): pl.pallas_call(lambda *refs: step_kernel(nz, ny, nx, *refs), out_shape=[j...  133 us
    pallas_call x1, Pallas kernels, layered(): pl.pallas_call(lambda *refs: finish_kernel(factor, *refs), grid=(4,), out...  4.7 us

profile of v2, /device:TPU:1, one launch (start us, length us, event | category | flops | bytes accessed | tf_op | source)
XLA Modules:
  0.0 138.0 jit_solution(9557406292849350981)
XLA Ops:
  0.6 132.6 %step.1 = (bf16[48,2048]{1,0:T(8,128)(2,1)}, bf16[48,2048]{1,0:T(8,128)(2,1)}, bf16[2,192,352]{2,1,0:T(8,128)(2,1)}, bf16[2,3,352,256]{3,2,1,0:T(8,128)(2,1)}) custom-call(bf16[704,256]{1,0:T(8,128)(2,1)} %bitcast.8, bf16[704,256]{1,0:T(8,128)(2,1)} %bitcast.9, bf16[704,256]{1,0:T(8,128)(2,1)} %refs_2_.1, bf16[48,2048]{1,0:T(8,128)(2,1)} %refs_3_.2, ...), custom_call_target="tpu_custom_call" | custom-call | tf_op jit(solution)/shard_map/step/pallas_call | solution.py:654
  133.3 4.7 %finish.1 = (f32[704,256]{1,0:T(8,128)}, f32[704,256]{1,0:T(8,128)}, f32[704,256]{1,0:T(8,128)}, bf16[192,704]{1,0:T(8,128)(2,1)}, bf16[48,2048]{1,0:T(8,128)(2,1)}, /*index=5*/bf16[48,2048]{1,0:T(8,128)(2,1)}) custom-call(bf16[2,3,352,256]{3,2,1,0:T(8,128)(2,1)} %get-tuple-element.16.refs_0_, f32[704,256]{1,0:T(8,128)} %bitcast.6, f32[704,256]{1,0:T(8,128)} %bitcast.7, ...), custom_call_target="tpu_custom_call" | custom-call | tf_op jit(solution)/shard_map/finish/pallas_call | solution.py:693
